TPU v7x, 32 devices: a whole 2x2x4 slice. The times are simulated.
32 devices in a mesh: sp: 4 (over z), dp: 8 (over y, x, core).
Axes of the slice: x: 2, y: 2, z: 4, core: 2. Of those that a mesh axis runs over, the one named last changes fastest.
Arguments:
- value_half: bfloat16 [8, 1536, 2048], P('dp', 'sp'), may hold values from -6 to 6
- gate_half: bfloat16 [8, 1536, 2048], P('dp', 'sp'), may hold values from -9 to 9
- conv_taps: bfloat16 [31, 2048], replicated, may hold values from -1 to 1
- norm_gain: float32 [2048], replicated, may hold values from 0.1 to 1.9
- norm_shift: float32 [2048], replicated, may hold values from -3 to 3
- out_weight: bfloat16 [2048, 2048], P('dp', 'sp'), may hold values from -0.125 to 0.125
Outputs:
- module_out: bfloat16 [8, 1536, 2048], P('dp', 'sp')
All inputs are finite; a program needn't handle non-finite values.
Results may differ from a plain program's by a relative error of at most 0.0064.
Values may be sent and summed in bfloat16 or wider, within the bound.
A program may use at most 64 MiB of HBM per device.

v0:
```python
import jax
import jax.numpy as jnp
from jax import lax
from jax.sharding import PartitionSpec as P

EPSILON = 1e-06


def passed_along(value, axis, steps):
    count = lax.axis_size(axis)
    initial, last = (max(0, -steps), min(count, count - steps))
    return lax.ppermute(value, axis, [(source, source + steps) for source in range(initial, last)])


def causal_mix(padded, conv_taps, length):
    tap_count = conv_taps.shape[0]
    running = jnp.zeros((length, padded.shape[1]), jnp.float32)
    for tap_index in range(tap_count):
        running = running + padded[tap_index : tap_index + length].astype(jnp.float32) * conv_taps[
            tap_index
        ].astype(jnp.float32)
    return running.astype(jnp.bfloat16)


def per_device(value_half, gate_half, conv_taps, norm_gain, norm_shift, out_weight):
    tap_count = conv_taps.shape[0]
    tok_rows = value_half.shape[1]
    gated = (
        value_half[0].astype(jnp.float32) * jax.nn.sigmoid(gate_half[0].astype(jnp.float32))
    ).astype(jnp.bfloat16)
    tail_rows = gated[tok_rows - (tap_count - 1) :]
    history = passed_along(tail_rows, "sp", 1)
    padded = jnp.concatenate([history, gated], 0)
    convolved = causal_mix(padded, conv_taps, tok_rows)
    widened = convolved.astype(jnp.float32)
    mean_row = jnp.mean(widened, axis=-1, keepdims=True)
    centered = widened - mean_row
    variance = jnp.mean(centered * centered, axis=-1, keepdims=True)
    normed = centered * lax.rsqrt(variance + EPSILON) * norm_gain + norm_shift
    activated = jax.nn.silu(normed).astype(jnp.bfloat16)
    row_block = lax.all_gather(out_weight, "sp", axis=1, tiled=True)
    projected = jnp.dot(
        activated,
        lax.all_gather(row_block, "dp", axis=0, tiled=True),
        preferred_element_type=jnp.float32,
    )
    return projected.astype(jnp.bfloat16)[None]


def solution(mesh):
    placed = (P("dp", "sp", None), P("dp", "sp", None), P(), P(), P(), P("dp", "sp"))
    return jax.shard_map(
        per_device, mesh=mesh, in_specs=placed, out_specs=P("dp", "sp", None), check_vma=False
    )
```

profile of v0, /device:TPU:0, one launch (start us, length us, event | category | flops | bytes accessed | tf_op | source)
XLA Modules:
  0.0 110.5 jit_solution(4330929815768049006)
XLA Ops:
  6.5 0.0 copy-start
  6.5 0.0 all-gather.3.cloned.1.call-start
  6.5 0.7 all-gather.3.cloned.1.call-update
  7.3 0.0 all-gather.5.cloned.1.call-start
  7.3 32.3 %all-gather.3.cloned.1.call-done = bf16[256,2048]{1,0:T(8,128)(2,1)} async-done(((bf16[256,512]{1,0:T(8,128)(2,1)}), bf16[256,2048]{1,0:T(8,128)(2,1)}) %all-gather.3.cloned.1.call-update) | async-done | bytes 1048592 | tf_op jit(solution)/shard_map/all_gather | solution.py:41
  39.6 0.0 all-gather.5.cloned.1.call-update
  39.7 2.8 %multiply_convert_fusion = bf16[1,384,2048]{2,1,0:T(8,128)(2,1)S(1)} fusion(bf16[1,384,2048]{2,1,0:T(8,128)(2,1)} %param.6, bf16[1,384,2048]{2,1,0:T(8,128)(2,1)} %param.7), kind=kLoop, calls=%fused_computation.42 | loop fusion | flops 5505024 | bytes 4718592 | tf_op jit(solution)/shard_map/convert_element_type | solution.py:30
  42.5 0.0 copy-start.1
  42.5 0.0 copy-start.2
  42.5 3.4 %collective-permute-start = (bf16[30,2048]{1,0:T(8,128)(2,1)S(1)}, bf16[30,2048]{1,0:T(8,128)(2,1)S(1)}, u32[]{:S(2)}, u32[]{:S(2)}) collective-permute-start(bf16[30,2048]{1,0:T(8,128)(2,1)S(1)} %slice_bitcast_fusion), channel_id=1, source_target_pairs={{0,8},{8,16},{16,24},{1,9},{9,17},{17,25},{2,10},{10,18},{18,26},{... | collective-permute-start | bytes 368648 | tf_op jit(solution)/shard_map/ppermute | solution.py:12
  45.9 0.0 copy-done
  45.9 0.1 slice_convert_fusion.30
  46.0 0.1 slice_convert_fusion.29
  46.1 2.3 %collective-permute-done = bf16[30,2048]{1,0:T(8,128)(2,1)S(1)} collective-permute-done((bf16[30,2048]{1,0:T(8,128)(2,1)S(1)}, bf16[30,2048]{1,0:T(8,128)(2,1)S(1)}, u32[]{:S(2)}, u32[]{:S(2)}) %collective-permute-start) | collective-permute-done | bytes 122912 | tf_op jit(solution)/shard_map/ppermute | solution.py:12
  48.4 14.3 %convert_reduce_fusion = (f32[384]{0:T(512)S(1)}, bf16[384,2048]{1,0:T(8,128)(2,1)S(1)}) fusion(f32[2048]{0:T(1024)S(1)} %bitcast.67, bf16[384,2048]{1,0:T(8,128)(2,1)S(1)} %bitcast.37, f32[2048]{0:T(1024)S(1)} %bitcast.68, bf16[30,2048]{1,0:T(8,128)(2,1)S(1)} %collective-permute-done, f32[2048]{0:T(1024)S(1)} %bitcast.39, f32[2048]{0:T(1024)S(1)} %bitcast.40, ...), kind=kLoop, calls=%fused_computation.30 | loop fusion | flops 145489536 | bytes 3524096 | tf_op jit(solution)/shard_map/reduce_sum | solution.py:36
  62.7 0.6 fusion.2
  63.2 31.9 %all-gather.5.cloned.1.call-done = bf16[2048,2048]{1,0:T(8,128)(2,1)} async-done(((bf16[256,2048]{1,0:T(8,128)(2,1)}), bf16[2048,2048]{1,0:T(8,128)(2,1)}) %all-gather.5.cloned.1.call-update) | async-done | bytes 8388624 | tf_op jit(solution)/shard_map/all_gather | solution.py:44
  95.2 0.0 copy-done.1
  95.2 0.0 copy-done.2
  95.2 8.5 %fusion.11 = bf16[1,384,2048]{2,1,0:T(8,128)(2,1)} fusion(bf16[2048,2048]{1,0:T(8,128)(2,1)} %all-gather.5.cloned.1.call-done, bf16[384,2048]{1,0:T(8,128)(2,1)S(1)} %get-tuple-element.6, f32[2048]{0:T(1024)S(1)} %copy-done.1, f32[2048]{0:T(1024)S(1)} %copy-done.2, f32[384]{0:T(512)S(1)} %add_rsqrt_fusion, f32[384]{0:T(512)S(1)} %broadcast_multiply_fusion), kind=kOutput, calls=%fused_computation.45 | convolution fusion | flops 3229876224 | bytes 11553792 | tf_op jit(solution)/shard_map/dot_general | solution.py:42
  (3 shorter events, 0.0 us)
Async XLA Ops:
  6.5 39.4 %copy-start = (bf16[31,2048]{1,0:T(8,128)(2,1)S(1)}, bf16[31,2048]{1,0:T(8,128)(2,1)}, u32[]{:S(2)}) copy-start(bf16[31,2048]{1,0:T(8,128)(2,1)} %param.8) | copy-start | bytes 380932
  6.5 33.1 %all-gather.3.cloned.1.call-start = ((), (), s32[]{:S(2)}) async-start(), calls=%async_computation | async-start | bytes 1310720 | tf_op jit(solution)/shard_map/all_gather | solution.py:41
  7.3 87.9 %all-gather.5.cloned.1.call-start = ((), (), s32[]{:S(2)}) async-start(), calls=%async_computation.1 | async-start | bytes 9437184 | tf_op jit(solution)/shard_map/all_gather | solution.py:44
  42.5 52.7 %copy-start.1 = (f32[2048]{0:T(1024)S(1)}, f32[2048]{0:T(1024)}, u32[]{:S(2)}) copy-start(f32[2048]{0:T(1024)} %param.10) | copy-start | bytes 24580
  42.5 52.7 %copy-start.2 = (f32[2048]{0:T(1024)S(1)}, f32[2048]{0:T(1024)}, u32[]{:S(2)}) copy-start(f32[2048]{0:T(1024)} %param.9) | copy-start | bytes 24580
  42.5 5.9 %collective-permute-start = (bf16[30,2048]{1,0:T(8,128)(2,1)S(1)}, bf16[30,2048]{1,0:T(8,128)(2,1)S(1)}, u32[]{:S(2)}, u32[]{:S(2)}) collective-permute-start(bf16[30,2048]{1,0:T(8,128)(2,1)S(1)} %slice_bitcast_fusion), channel_id=1, source_target_pairs={{0,8},{8,16},{16,24},{1,9},{9,17},{17,25},{2,10},{10,18},{18,26},{... | collective-permute-start | bytes 368648 | tf_op jit(solution)/shard_map/ppermute | solution.py:12
Sparse Core Ops, SparseCore 0:
  8.9 30.6 all-gather.2
  41.5 53.6 all-gather.4
where the time goes:
time: 111 us
  waiting for transfers between devices  67.3 us (61%)
  other arithmetic  17.8 us (16%)
  between operations  13.5 us (12%)
  matrix products  8.49 us (8%)
  starting transfers between devices  3.4 us (3%)
    all_gather x1, waiting for transfers between devices, per_device(): row_block = lax.all_gather(out_weight, 'sp', axis=1, tiled=True)  32.3 us
    all_gather x1, waiting for transfers between devices, per_device(): lax.all_gather(row_block, 'dp', axis=0, tiled=True)  31.9 us
    reduce_sum x1, other arithmetic, per_device(): mean_row = jnp.mean(widened, axis=-1, keepdims=True)  14.3 us
    dot_general x1, matrix products, per_device(): jnp.dot(activated, lax.all_gather(row_block, 'dp', axis=0, tiled=True), p...  8.49 us
    ppermute x1, starting transfers between devices, passed_along(): lax.ppermute(value, axis, [(source, source + steps) for source in range(i...  3.36 us
    convert_element_type x1, other arithmetic, per_device(): gated = (value_half[0].astype(jnp.float32) * jax.nn.sigmoid(gate_half[0]....  2.79 us
    ppermute x1, waiting for transfers between devices, passed_along(): lax.ppermute(value, axis, [(source, source + steps) for source in range(i...  2.29 us
  transfers between devices with their start and end apart: 3, of which 3 were waited for; matrix products, arithmetic and copies ran while one was open for 16% of the time, Pallas kernels for 0%

commit v1 on v0

--- a/solution.py
+++ b/solution.py
@@ -38,7 +38,13 @@
     variance = jnp.mean(centered * centered, axis=-1, keepdims=True)
     normed = centered * lax.rsqrt(variance + EPSILON) * norm_gain + norm_shift
     activated = jax.nn.silu(normed).astype(jnp.bfloat16)
-    row_block = lax.all_gather(out_weight, "sp", axis=1, tiled=True)
+    count_2 = lax.axis_size("sp")
+    moving, blocks = (out_weight, [out_weight])
+    for _ in range(count_2 - 1):
+        moving = lax.ppermute(moving, "sp", [(i, (i + 1) % count_2) for i in range(count_2)])
+        blocks.insert(0, moving)
+    line = jnp.concatenate(blocks, axis=1)
+    row_block = jnp.roll(line, (lax.axis_index("sp") + 1) * out_weight.shape[1], axis=1)
     projected = jnp.dot(
         activated,
         lax.all_gather(row_block, "dp", axis=0, tiled=True),

time: 111 us -> 111 us (level)
  local copies, waits for them, and re-layouts: 0.05 us -> 6.63 us
  waiting for transfers between devices: 67.3 us -> 61.3 us
  other arithmetic: 17.8 us -> 15.9 us
    all_gather x1 -> x0, waiting for transfers between devices: 32.3 us -> none  [per_device(): row_block = lax.all_gather(out_weight, 'sp', axis=1, tiled=True)]
    ppermute x0 -> x3, waiting for transfers between devices: none -> 26.3 us  [per_device(): lax.ppermute(moving, 'sp', [(i, (i + 1) % count_2) for i in range(count_2)])]
    unnamed x6 -> x27, local copies, waits for them, and re-layouts: 0.02 us -> 5.53 us
    ppermute x0 -> x3, starting transfers between devices: none -> 3.06 us  [per_device(): lax.ppermute(moving, 'sp', [(i, (i + 1) % count_2) for i in range(count_2)])]
    ppermute x1, starting transfers between devices: 3.36 us -> 1.3 us  [passed_along(): lax.ppermute(value, axis, [(source, source + steps) for source in range(i...]
    convert_element_type x1, other arithmetic: 2.79 us -> 0.86 us  [per_device(): gated = (value_half[0].astype(jnp.float32) * jax.nn.sigmoid(gate_half[0]....]
  transfers between devices with their start and end apart: 3 -> 5, of which waited for: 3 -> 5; matrix products, arithmetic and copies ran while one was open for 16% -> 14% of each run, Pallas kernels for 0% -> 0%
where the time goes in v1:
time: 111 us; the launch traced here: 110 us
  waiting for transfers between devices  61.3 us (55%)
  other arithmetic  15.9 us (14%)
  between operations  13.6 us (12%)
  matrix products  8.5 us (8%)
  local copies, waits for them, and re-layouts  6.63 us (6%)
  starting transfers between devices  4.36 us (4%)
    all_gather x1, waiting for transfers between devices, per_device(): lax.all_gather(row_block, 'dp', axis=0, tiled=True)  32.7 us
    ppermute x3, waiting for transfers between devices, per_device(): lax.ppermute(moving, 'sp', [(i, (i + 1) % count_2) for i in range(count_2)])  26.3 us
    reduce_sum x1, other arithmetic, per_device(): mean_row = jnp.mean(widened, axis=-1, keepdims=True)  14.3 us
    dot_general x1, matrix products, per_device(): jnp.dot(activated, lax.all_gather(row_block, 'dp', axis=0, tiled=True), p...  8.5 us
    unnamed x27, local copies, waits for them, and re-layouts  5.53 us
    ppermute x3, starting transfers between devices, per_device(): lax.ppermute(moving, 'sp', [(i, (i + 1) % count_2) for i in range(count_2)])  3.06 us
    ppermute x1, waiting for transfers between devices, passed_along(): lax.ppermute(value, axis, [(source, source + steps) for source in range(i...  2.29 us
  transfers between devices with their start and end apart: 5, of which 5 were waited for; matrix products, arithmetic and copies ran while one was open for 14% of the time, Pallas kernels for 0%

profile of v1, /device:TPU:0, one launch (start us, length us, event | category | flops | bytes accessed | tf_op | source)
XLA Modules:
  0.0 110.3 jit_solution(1112039941945536667)
XLA Ops:
  6.5 0.0 all-gather.2.cloned.1.call-start
  6.5 3.1 %collective-permute-start.1 = (bf16[256,512]{1,0:T(8,128)(2,1)}, bf16[256,512]{1,0:T(8,128)(2,1)S(1)}, u32[]{:S(2)}, u32[]{:S(2)}) collective-permute-start(bf16[256,512]{1,0:T(8,128)(2,1)} %param.11), channel_id=1, source_target_pairs={{0,8},{8,16},{16,24},{24,0},{1,9},{9,17},{17,25},{25,1},{2,10},{10... | collective-permute-start | bytes 786440 | tf_op jit(solution)/shard_map/ppermute | solution.py:44
  9.6 8.6 %collective-permute-done.1 = bf16[256,512]{1,0:T(8,128)(2,1)S(1)} collective-permute-done((bf16[256,512]{1,0:T(8,128)(2,1)}, bf16[256,512]{1,0:T(8,128)(2,1)S(1)}, u32[]{:S(2)}, u32[]{:S(2)}) %collective-permute-start.1) | collective-permute-done | bytes 262176 | tf_op jit(solution)/shard_map/ppermute | solution.py:44
  18.2 0.7 copy-done.3
  18.9 0.0 collective-permute-start.2
  18.9 9.3 %collective-permute-done.2 = bf16[256,512]{1,0:T(8,128)(2,1)S(1)} collective-permute-done((bf16[256,512]{1,0:T(8,128)(2,1)S(1)}, bf16[256,512]{1,0:T(8,128)(2,1)S(1)}, u32[]{:S(2)}, u32[]{:S(2)}) %collective-permute-start.2) | collective-permute-done | bytes 262176 | tf_op jit(solution)/shard_map/ppermute | solution.py:44
  28.2 0.0 collective-permute-start.3
  28.2 8.4 %collective-permute-done.3 = bf16[256,512]{1,0:T(8,128)(2,1)S(1)} collective-permute-done((bf16[256,512]{1,0:T(8,128)(2,1)S(1)}, bf16[256,512]{1,0:T(8,128)(2,1)S(1)}, u32[]{:S(2)}, u32[]{:S(2)}) %collective-permute-start.3) | collective-permute-done | bytes 262176 | tf_op jit(solution)/shard_map/ppermute | solution.py:44
  36.6 0.0 copy-done.5
  36.6 0.7 copy-done.6
  37.3 0.0 copy-start
  37.3 0.0 copy-start.1
  37.3 1.1 %constant_dynamic-update-slice_fusion.5 = bf16[256,4096]{1,0:T(8,128)(2,1)S(1)} fusion(bf16[256,4096]{1,0:T(8,128)(2,1)S(1)} %constant_dynamic-update-slice_fusion.6, bf16[256,512]{1,0:T(8,128)(2,1)} %copy-done.3), kind=kLoop, calls=%fused_computation.93 | loop fusion | bytes 524288
  38.5 1.0 constant_dynamic-update-slice_fusion.4
  39.5 1.0 constant_dynamic-update-slice_fusion.3
  40.4 1.0 constant_dynamic-update-slice_fusion.2
  41.4 0.0 copy-done.4
  41.5 1.0 constant_dynamic-slice_fusion
  42.6 0.0 all-gather.2.cloned.1.call-update
  42.6 0.0 copy-done
  42.6 0.0 copy-done.1
  42.6 0.9 multiply_convert_fusion
  43.5 0.0 copy-start.8
  43.5 0.0 copy-start.9
  43.5 1.3 %collective-permute-start = (bf16[30,2048]{1,0:T(8,128)(2,1)S(1)}, bf16[30,2048]{1,0:T(8,128)(2,1)S(1)}, u32[]{:S(2)}, u32[]{:S(2)}) collective-permute-start(bf16[30,2048]{1,0:T(8,128)(2,1)S(1)} %slice_bitcast_fusion), channel_id=1, source_target_pairs={{0,8},{8,16},{16,24},{1,9},{9,17},{17,25},{2,10},{10,18},{18,26},{... | collective-permute-start | bytes 368648 | tf_op jit(solution)/shard_map/ppermute | solution.py:12
  44.9 0.1 slice_convert_fusion.30
  45.0 0.1 slice_convert_fusion.29
  45.1 2.3 %collective-permute-done = bf16[30,2048]{1,0:T(8,128)(2,1)S(1)} collective-permute-done((bf16[30,2048]{1,0:T(8,128)(2,1)S(1)}, bf16[30,2048]{1,0:T(8,128)(2,1)S(1)}, u32[]{:S(2)}, u32[]{:S(2)}) %collective-permute-start) | collective-permute-done | bytes 122912 | tf_op jit(solution)/shard_map/ppermute | solution.py:12
  47.3 14.3 %convert_reduce_fusion = (f32[384]{0:T(512)S(1)}, bf16[384,2048]{1,0:T(8,128)(2,1)S(1)}) fusion(f32[2048]{0:T(1024)S(1)} %bitcast.67, bf16[384,2048]{1,0:T(8,128)(2,1)S(1)} %bitcast.37, f32[2048]{0:T(1024)S(1)} %bitcast.68, bf16[30,2048]{1,0:T(8,128)(2,1)S(1)} %collective-permute-done, f32[2048]{0:T(1024)S(1)} %bitcast.39, f32[2048]{0:T(1024)S(1)} %bitcast.40, ...), kind=kLoop, calls=%fused_computation.30 | loop fusion | flops 145489536 | bytes 3524096 | tf_op jit(solution)/shard_map/reduce_sum | solution.py:36
  61.6 0.6 fusion.2
  62.2 32.7 %all-gather.2.cloned.1.call-done = bf16[2048,2048]{1,0:T(8,128)(2,1)} async-done(((bf16[256,2048]{1,0:T(8,128)(2,1)}), bf16[2048,2048]{1,0:T(8,128)(2,1)}) %all-gather.2.cloned.1.call-update) | async-done | bytes 8388624 | tf_op jit(solution)/shard_map/all_gather | solution.py:50
  94.9 8.5 %fusion.11 = bf16[1,384,2048]{2,1,0:T(8,128)(2,1)} fusion(bf16[2048,2048]{1,0:T(8,128)(2,1)} %all-gather.2.cloned.1.call-done, bf16[384,2048]{1,0:T(8,128)(2,1)S(1)} %get-tuple-element.6, f32[2048]{0:T(1024)S(1)} %copy-done.8, f32[2048]{0:T(1024)S(1)} %copy-done.9, f32[384]{0:T(512)S(1)} %add_rsqrt_fusion, f32[384]{0:T(512)S(1)} %broadcast_multiply_fusion), kind=kOutput, calls=%fused_computation.45 | convolution fusion | flops 3229876224 | bytes 11553792 | tf_op jit(solution)/shard_map/dot_general | solution.py:48
  (17 shorter events, 0.2 us)
Async XLA Ops:
  6.5 34.9 %copy-start.2 = (bf16[256,512]{1,0:T(8,128)(2,1)S(1)}, bf16[256,512]{1,0:T(8,128)(2,1)}, u32[]{:S(2)}) copy-start(bf16[256,512]{1,0:T(8,128)(2,1)} %param.11) | copy-start | bytes 786436
  6.5 88.4 %all-gather.2.cloned.1.call-start = ((), (), s32[]{:S(2)}) async-start(), calls=%async_computation | async-start | bytes 9437184 | tf_op jit(solution)/shard_map/all_gather | solution.py:50
  6.5 11.7 %collective-permute-start.1 = (bf16[256,512]{1,0:T(8,128)(2,1)}, bf16[256,512]{1,0:T(8,128)(2,1)S(1)}, u32[]{:S(2)}, u32[]{:S(2)}) collective-permute-start(bf16[256,512]{1,0:T(8,128)(2,1)} %param.11), channel_id=1, source_target_pairs={{0,8},{8,16},{16,24},{24,0},{1,9},{9,17},{17,25},{25,1},{2,10},{10... | collective-permute-start | bytes 786440 | tf_op jit(solution)/shard_map/ppermute | solution.py:44
  18.2 0.7 copy-start.3
  18.9 9.3 %collective-permute-start.2 = (bf16[256,512]{1,0:T(8,128)(2,1)S(1)}, bf16[256,512]{1,0:T(8,128)(2,1)S(1)}, u32[]{:S(2)}, u32[]{:S(2)}) collective-permute-start(bf16[256,512]{1,0:T(8,128)(2,1)S(1)} %collective-permute-done.1), channel_id=1, source_target_pairs={{0,8},{8,16},{16,24},{24,0},{1,9},{9,17},{17,25},{25,1},{2,10},{10... | collective-permute-start | bytes 786440 | tf_op jit(solution)/shard_map/ppermute | solution.py:44
  28.2 8.4 %copy-start.5 = (bf16[256,512]{1,0:T(8,128)(2,1)}, bf16[256,512]{1,0:T(8,128)(2,1)S(1)}, u32[]{:S(2)}) copy-start(bf16[256,512]{1,0:T(8,128)(2,1)S(1)} %collective-permute-done.2) | copy-start | bytes 786436
  28.2 8.4 %collective-permute-start.3 = (bf16[256,512]{1,0:T(8,128)(2,1)S(1)}, bf16[256,512]{1,0:T(8,128)(2,1)S(1)}, u32[]{:S(2)}, u32[]{:S(2)}) collective-permute-start(bf16[256,512]{1,0:T(8,128)(2,1)S(1)} %collective-permute-done.2), channel_id=1, source_target_pairs={{0,8},{8,16},{16,24},{24,0},{1,9},{9,17},{17,25},{25,1},{2,10},{10... | collective-permute-start | bytes 786440 | tf_op jit(solution)/shard_map/ppermute | solution.py:44
  28.2 13.3 %copy-start.4 = (bf16[256,512]{1,0:T(8,128)(2,1)S(1)}, bf16[256,512]{1,0:T(8,128)(2,1)}, u32[]{:S(2)}) copy-start(bf16[256,512]{1,0:T(8,128)(2,1)} %copy-done.3) | copy-start | bytes 786436
  36.6 0.7 copy-start.6
  37.3 5.3 %copy-start = (bf16[1,384,2048]{2,1,0:T(8,128)(2,1)S(1)}, bf16[1,384,2048]{2,1,0:T(8,128)(2,1)}, u32[]{:S(2)}) copy-start(bf16[1,384,2048]{2,1,0:T(8,128)(2,1)} %param.6) | copy-start | bytes 4718596
  37.3 5.3 %copy-start.1 = (bf16[1,384,2048]{2,1,0:T(8,128)(2,1)S(1)}, bf16[1,384,2048]{2,1,0:T(8,128)(2,1)}, u32[]{:S(2)}) copy-start(bf16[1,384,2048]{2,1,0:T(8,128)(2,1)} %param.7) | copy-start | bytes 4718596
  42.6 2.3 %copy-start.7 = (bf16[31,2048]{1,0:T(8,128)(2,1)S(1)}, bf16[31,2048]{1,0:T(8,128)(2,1)}, u32[]{:S(2)}) copy-start(bf16[31,2048]{1,0:T(8,128)(2,1)} %param.8) | copy-start | bytes 380932
  43.5 51.4 %copy-start.8 = (f32[2048]{0:T(1024)S(1)}, f32[2048]{0:T(1024)}, u32[]{:S(2)}) copy-start(f32[2048]{0:T(1024)} %param.10) | copy-start | bytes 24580
  43.5 51.4 %copy-start.9 = (f32[2048]{0:T(1024)S(1)}, f32[2048]{0:T(1024)}, u32[]{:S(2)}) copy-start(f32[2048]{0:T(1024)} %param.9) | copy-start | bytes 24580
  43.5 3.8 %collective-permute-start = (bf16[30,2048]{1,0:T(8,128)(2,1)S(1)}, bf16[30,2048]{1,0:T(8,128)(2,1)S(1)}, u32[]{:S(2)}, u32[]{:S(2)}) collective-permute-start(bf16[30,2048]{1,0:T(8,128)(2,1)S(1)} %slice_bitcast_fusion), channel_id=1, source_target_pairs={{0,8},{8,16},{16,24},{1,9},{9,17},{17,25},{2,10},{10,18},{18,26},{... | collective-permute-start | bytes 368648 | tf_op jit(solution)/shard_map/ppermute | solution.py:12
Sparse Core Ops, SparseCore 0:
  42.7 52.1 all-gather.1
